TPU v7x, 32 devices: a whole 2x2x4 slice. The times are simulated.
32 devices in a mesh: sp: 4 (over y, x), tp: 8 (over z, core).
Axes of the slice: x: 2, y: 2, z: 4, core: 2. Of those that a mesh axis runs over, the one named last changes fastest.
Arguments:
- tokens: bfloat16 [2, 512, 4096], P(None, 'sp', 'tp'), may hold values from -6 to 6
- key_matrix: bfloat16 [4096, 4096], P(None, 'tp'), may hold values from -0.09375 to 0.09375
- value_matrix: bfloat16 [4096, 4096], P(None, 'tp'), may hold values from -0.375 to 0.375
- gate_matrix: bfloat16 [4096, 64], replicated, may hold values from -0.09375 to 0.09375
- head_decay_rate: float32 [32], P('tp'), may hold values from 0 to 1, as said below
- extra_log_decay: float32 [2, 32, 512], P(None, 'tp', 'sp'), may hold values from -3 to 0, as said below
- next_token_query: bfloat16 [2, 4096], P(None, 'tp'), may hold values from -6 to 6
- next_token_key: bfloat16 [2, 4096], P(None, 'tp'), may hold values from -6 to 6
- next_token_value: bfloat16 [2, 32, 128], P(None, 'tp', 'sp'), may hold values from -6 to 6
- next_write_strength: float32 [2, 32], P(None, 'tp'), may hold values from 0.05 to 1
- read_norm_gain: float32 [128], P('sp'), may hold values from 0.1 to 1.9
Outputs:
- state_cache: bfloat16 [2, 32, 128, 128], P(None, 'tp', None, 'sp')
- first_read: bfloat16 [2, 32, 128], P(None, 'tp', 'sp')
Inputs may be any that keep to these rules, and one draw needn't show every extreme that they name: `head_decay_rate`: positive. `extra_log_decay`: never positive.
All inputs are finite; a program needn't handle non-finite values.
Results may differ from a plain program's by a relative error of at most 0.013.
Values may be sent and summed in bfloat16 or wider, within the bound.
A program may use at most 64 MiB of HBM per device.

v0:
```python
import jax
import jax.numpy as jnp
from jax import lax
from jax.sharding import PartitionSpec as P

DV = 128
exact_mode = lax.Precision.HIGHEST
strength_offset = 5.0


def unit_rows(matrix):
    return matrix * lax.rsqrt(jnp.sum(matrix * matrix, axis=-1, keepdims=True) + 1e-06)


def nilpotent_inverse(mixing):
    extent = mixing.shape[-1]
    result = jnp.zeros_like(mixing) + jnp.eye(extent, dtype=jnp.float32)
    powered = -mixing
    covered = 1
    while covered < extent:
        product = lax.optimization_barrier(
            jnp.einsum("...ij,...jk->...ik", result, powered, precision=exact_mode)
        )
        result = result + product
        powered = jnp.einsum("...ij,...jk->...ik", powered, powered, precision=exact_mode)
        covered = covered * 2
    return result


def block_terms(unit_keys, values, decay_logarithm, strength):
    extent = unit_keys.shape[-2]
    lower = jnp.tril(jnp.ones((extent, extent), jnp.bool_))
    strict = jnp.tril(jnp.ones((extent, extent), jnp.bool_), -1)
    running = jnp.cumsum(decay_logarithm, axis=-1)
    spread = running[..., :, None] - running[..., None, :]
    within = jnp.where(lower, jnp.exp(jnp.where(lower, spread, 0.0)), 0.0)
    scaled = unit_keys * strength[..., None]
    mixing = jnp.where(
        strict,
        jnp.einsum("...id,...jd->...ij", scaled, unit_keys, precision=exact_mode) * within,
        0.0,
    )
    inverse = nilpotent_inverse(mixing)
    writes = jnp.einsum(
        "...ij,...je->...ie", inverse, values * strength[..., None], precision=exact_mode
    )
    erases = jnp.einsum(
        "...ij,...jd->...id", inverse, scaled * jnp.exp(running)[..., None], precision=exact_mode
    )
    final_log = running[..., -1]
    carried = unit_keys * jnp.exp(final_log[..., None] - running)[..., None]
    return (writes, erases, carried, final_log)


def split_blocks(array, block_count):
    shaped = array.reshape(
        array.shape[:2] + (block_count, array.shape[2] // block_count) + array.shape[3:]
    )
    return jnp.moveaxis(shaped, 2, 0)


def local(
    tokens,
    key_matrix,
    value_matrix,
    gate_matrix,
    head_decay_rate,
    extra_log_decay,
    next_token_query,
    next_token_key,
    next_token_value,
    next_write_strength,
    read_norm_gain,
):
    sequences, positions, _ = tokens.shape
    local_heads = head_decay_rate.shape[0]
    key_width = key_matrix.shape[1] // local_heads
    value_width = value_matrix.shape[1] // local_heads
    all_heads = gate_matrix.shape[1] // 2
    group_size = lax.axis_size("sp")
    column_share = value_width // group_size
    first_head = lax.axis_index("tp") * local_heads
    decay_cols = lax.dynamic_slice_in_dim(gate_matrix, first_head, local_heads, 1)
    strength_cols = lax.dynamic_slice_in_dim(gate_matrix, all_heads + first_head, local_heads, 1)
    gate_cols = jnp.concatenate([decay_cols, strength_cols], axis=1)
    row_count = sequences * positions
    incoming = lax.all_gather(tokens, "tp", axis=2, tiled=True)
    span_width = incoming.shape[2]
    flat_rows = incoming.reshape(row_count, span_width)
    products = lax.optimization_barrier(
        (
            jnp.dot(flat_rows, key_matrix, preferred_element_type=jnp.float32),
            jnp.dot(flat_rows, value_matrix, preferred_element_type=jnp.float32),
            jnp.dot(flat_rows, gate_cols, preferred_element_type=jnp.float32),
        )
    )
    key_sum = products[0]
    value_sum = products[1]
    gate_pre = products[2]
    key_float = lax.optimization_barrier(key_sum.astype(jnp.bfloat16)).astype(jnp.float32)
    value_float = lax.optimization_barrier(value_sum.astype(jnp.bfloat16)).astype(jnp.float32)
    unit_keys = unit_rows(
        key_float.reshape(sequences, positions, local_heads, key_width).transpose(0, 2, 1, 3)
    )
    values = value_float.reshape(sequences, positions, local_heads, value_width).transpose(
        0, 2, 1, 3
    )
    gate_projected = gate_pre.reshape(sequences, positions, 2 * local_heads).transpose(0, 2, 1)
    decay_logarithm = (
        -head_decay_rate[None, :, None] * jax.nn.softplus(gate_projected[:, :local_heads])
        + extra_log_decay
    )
    strength = jax.nn.sigmoid(gate_projected[:, local_heads:] - strength_offset)
    block_count = positions // min(64, positions)
    block_parts = block_terms(
        split_blocks(unit_keys, block_count),
        split_blocks(values, block_count),
        split_blocks(decay_logarithm, block_count),
        split_blocks(strength, block_count),
    )
    identity = jnp.zeros((sequences, local_heads, key_width, key_width), jnp.float32) + jnp.eye(
        key_width, dtype=jnp.float32
    )
    start_map = jnp.concatenate(
        [identity, jnp.zeros((sequences, local_heads, key_width, value_width), jnp.float32)],
        axis=-1,
    )

    def advance(current, block_part):
        writes, erases, carried, final_log = block_part
        padded = jnp.concatenate(
            [jnp.zeros(writes.shape[:-1] + (key_width,), jnp.float32), writes], axis=-1
        )
        removed = lax.optimization_barrier(
            jnp.einsum("shcd,shde->shce", erases, current, precision=exact_mode)
        )
        fresh = padded - removed
        added = lax.optimization_barrier(
            jnp.einsum("shcd,shce->shde", carried, fresh, precision=exact_mode)
        )
        current = current * jnp.exp(final_log)[..., None, None] + added
        return (current, None)

    local_map, _ = lax.scan(advance, start_map, block_parts)
    carry_map = local_map[..., :key_width]
    write_map = local_map[..., key_width:]
    carry_copies = jnp.broadcast_to(carry_map[None], (group_size,) + carry_map.shape)
    write_parts = jnp.moveaxis(
        write_map.reshape(sequences, local_heads, key_width, group_size, column_share), 3, 0
    )
    carries = lax.all_to_all(carry_copies, "sp", split_axis=0, concat_axis=0, tiled=True)
    write_cols = lax.all_to_all(write_parts, "sp", split_axis=0, concat_axis=0, tiled=True)

    def fold_step(current, block_map):
        moved = lax.optimization_barrier(
            jnp.einsum("shij,shje->shie", block_map[0], current, precision=exact_mode)
        )
        return (moved + block_map[1], None)

    begin_state = jnp.zeros(write_cols.shape[1:], jnp.float32)
    folded, _ = lax.scan(fold_step, begin_state, (carries, write_cols))
    query_rows = next_token_query.astype(jnp.float32).reshape(sequences, local_heads, key_width)
    unit_new = unit_rows(
        next_token_key.astype(jnp.float32).reshape(sequences, local_heads, key_width)
    )
    value_rows = next_token_value.astype(jnp.float32)
    key_read = jnp.einsum("shd,shde->she", unit_new, folded, precision=exact_mode)
    query_read = jnp.einsum("shd,shde->she", query_rows, folded, precision=exact_mode)
    intersection = jnp.sum(query_rows * unit_new, axis=-1)
    read_raw = query_read + (next_write_strength * intersection)[..., None] * (
        value_rows - key_read
    )
    square_total = lax.psum(jnp.sum(read_raw * read_raw, axis=-1, keepdims=True), "sp")
    first_read = read_raw * lax.rsqrt(square_total / DV + 1e-06) * read_norm_gain
    return (folded.astype(jnp.bfloat16), first_read.astype(jnp.bfloat16))


def solution(mesh):
    in_specs = (
        P(None, "sp", "tp"),
        P(None, "tp"),
        P(None, "tp"),
        P(),
        P("tp"),
        P(None, "tp", "sp"),
        P(None, "tp"),
        P(None, "tp"),
        P(None, "tp", "sp"),
        P(None, "tp"),
        P("sp"),
    )
    out_specs = (P(None, "tp", None, "sp"), P(None, "tp", "sp"))
    return jax.shard_map(local, mesh=mesh, in_specs=in_specs, out_specs=out_specs, check_vma=False)
```

profile of v0, /device:TPU:0, one launch (start us, length us, event | category | flops | bytes accessed | tf_op | source)
XLA Modules:
  0.0 130.1 jit_solution(6070156353231956708)
XLA Ops:
  7.2 0.7 all-gather.2.cloned.1.call-update
  7.9 0.7 neg.14
  8.8 0.9 constant_dynamic-slice_fusion.2
  9.7 31.8 %all-gather.2.cloned.1.call-done = bf16[2,128,4096]{2,1,0:T(8,128)(2,1)} async-done(((bf16[2,128,512]{2,1,0:T(8,128)(2,1)}), bf16[2,128,4096]{2,1,0:T(8,128)(2,1)}) %all-gather.2.cloned.1.call-update) | async-done | bytes 2097168 | tf_op jit(solution)/shard_map/all_gather | solution.py:87
  41.5 4.2 %fusion.52 = bf16[256,512]{1,0:T(8,128)(2,1)S(1)} fusion(bf16[256,4096]{1,0:T(8,128)(2,1)} %bitcast.96, bf16[4096,512]{1,0:T(8,128)(2,1)} %param.16), kind=kOutput, calls=%fused_computation.86 | convolution fusion | flops 1073741824 | bytes 6553600 | tf_op jit(solution)/shard_map/dot_general | solution.py:92
  46.2 1.2 fusion.53
  48.2 1.1 reduce_window_sum.11
  51.0 1.0 fusion.22
  53.9 0.7 fusion.30
  55.2 0.7 fusion.38
  58.0 0.7 fusion.59
  58.8 0.7 fusion.61
  59.5 0.7 fusion.24
  60.1 0.7 fusion.26
  60.8 4.5 %while.21 = (s32[]{:T(128)}, f32[2,4,128,256]{3,2,1,0:T(8,128)S(1)}, f32[2,2,4]{2,1,0:T(2,128)S(1)}, f32[2,2,4,64,128]{4,3,0,2,1:T(8,128)S(1)}, f32[2,2,4,64,128...) while((s32[]{:T(128)}, f32[2,4,128,256]{3,2,1,0:T(8,128)S(1)}, ...), condition=%wide.region_3.4_spmd, body=%wide.region_2.3_spmd.sunk | while | flops 403308544 | bytes 7602365 | solution.py:144
  61.0 0.7 fusion.107
  61.8 1.1 fusion.108
  63.2 0.7 fusion.107
  64.0 1.1 fusion.108
  65.7 0.8 copy.38
  66.6 3.6 %all-to-all-start.1 = ((f32[4,2,4,128,32]{3,4,2,1,0:T(8,128)}), f32[4,2,4,128,32]{3,4,2,1,0:T(8,128)S(1)}, u32[]{:S(2)}, u32[]{:S(2)}) async-start(f32[4,2,4,128,32]{3,4,2,1,0:T(8,128)} %copy.38), calls=%async_computation.1 | async-start | bytes 1048576 | tf_op jit(solution)/shard_map/all_to_all | solution.py:152
  70.3 8.5 %all-to-all-done.1 = f32[4,2,4,128,32]{3,4,2,1,0:T(8,128)S(1)} async-done(((f32[4,2,4,128,32]{3,4,2,1,0:T(8,128)}), f32[4,2,4,128,32]{3,4,2,1,0:T(8,128)S(1)}, u32[]{:S(2)}, u32[]{:S(2)}) %all-to-all-start.1) | async-done | bytes 524320 | tf_op jit(solution)/shard_map/all_to_all | solution.py:152
  78.7 1.6 %broadcast_in_dim.51 = f32[4,2,4,128,128]{4,3,2,1,0:T(8,128)} broadcast(f32[2,4,128,128]{3,2,1,0:T(8,128)S(1)} %slice.18), dimensions={1,2,3,4} | broadcast | bytes 2621440 | tf_op jit(solution)/shard_map/broadcast_in_dim | solution.py:147
  80.3 3.7 %all-to-all-start = ((f32[4,2,4,128,128]{4,3,2,1,0:T(8,128)}), f32[4,2,4,128,128]{4,3,2,1,0:T(8,128)S(1)}, u32[]{:S(2)}, u32[]{:S(2)}) async-start(f32[4,2,4,128,128]{4,3,2,1,0:T(8,128)} %broadcast_in_dim.51), calls=%async_computation | async-start | bytes 4194304 | tf_op jit(solution)/shard_map/all_to_all | solution.py:151
  84.4 24.1 %all-to-all-done = f32[4,2,4,128,128]{4,3,2,1,0:T(8,128)S(1)} async-done(((f32[4,2,4,128,128]{4,3,2,1,0:T(8,128)}), f32[4,2,4,128,128]{4,3,2,1,0:T(8,128)S(1)}, u32[]{:S(2)}, u32[]{:S(2)}) %all-to-all-start) | async-done | bytes 2097184 | tf_op jit(solution)/shard_map/all_to_all | solution.py:151
  108.5 3.9 %while.22 = (s32[]{:T(128)}, f32[2,4,128,32]{2,3,1,0:T(8,128)S(1)}, f32[4,2,4,128,128]{4,3,2,1,0:T(8,128)S(1)}, f32[4,2,4,128,32]{3,4,2,1,0:T(8,128)S(1)}, s32[]{:T(128)}, /*index=5*/s32[]{:T(128)}) while((s32[]{:T(128)}, f32[2,4,128,32]{2,3,1,0:T(8,128)S(1)}, f32[4,2,4,128,128]{4,3,2,1,0:T(8,128)S(1)}, ...), condition=%wide.region_5.6_spmd.clone, body=%wide.region_4.5_spmd.clone.sunk | while | flops 50397184 | bytes 1179735 | solution.py:161
  108.5 0.9 fusion.112
  109.5 0.9 fusion.112
  110.4 0.9 fusion.112
  111.4 0.9 fusion.112
  113.7 8.9 %psum.7 = f32[2,4,1]{1,0,2:T(2,128)S(1)} all-reduce(f32[2,4,1]{1,0,2:T(2,128)S(1)} %bitcast.111), channel_id=1, replica_groups=mesh['sp'=4,'tp'=8] {'sp'}, use_global_device_ids=true, to_apply=%region_9.10 | all-reduce | flops 8 | bytes 64 | tf_op jit(solution)/shard_map/psum | solution.py:173
  122.6 0.7 multiply_convert_fusion
  (75 shorter events, 10.7 us)
Async XLA Ops:
  7.2 34.3 %all-gather.2.cloned.1.call-start = ((), (), s32[]{:S(2)}) async-start(), calls=%async_computation.2 | async-start | bytes 2359296 | tf_op jit(solution)/shard_map/all_gather | solution.py:87
  41.5 4.2 %copy-start = (bf16[2,128,4096]{2,1,0:T(8,128)(2,1)S(1)}, bf16[2,128,4096]{2,1,0:T(8,128)(2,1)}, u32[]{:S(2)}) copy-start(bf16[2,128,4096]{2,1,0:T(8,128)(2,1)} %all-gather.2.cloned.1.call-done) | copy-start | bytes 6291460
  41.5 4.7 %copy-start.7 = (bf16[4096,512]{1,0:T(8,128)(2,1)S(1)}, bf16[4096,512]{1,0:T(8,128)(2,1)}, u32[]{:S(2)}) copy-start(bf16[4096,512]{1,0:T(8,128)(2,1)} %param.17) | copy-start | bytes 12582916
  47.4 0.7 copy-start.3
  66.6 12.1 %all-to-all-start.1 = ((f32[4,2,4,128,32]{3,4,2,1,0:T(8,128)}), f32[4,2,4,128,32]{3,4,2,1,0:T(8,128)S(1)}, u32[]{:S(2)}, u32[]{:S(2)}) async-start(f32[4,2,4,128,32]{3,4,2,1,0:T(8,128)} %copy.38), calls=%async_computation.1 | async-start | bytes 1048576 | tf_op jit(solution)/shard_map/all_to_all | solution.py:152
  80.3 3.8 %copy-start.1 = (bf16[2,512]{1,0:T(2,128)(2,1)S(1)}, bf16[2,512]{1,0:T(2,128)(2,1)}, u32[]{:S(2)}) copy-start(bf16[2,512]{1,0:T(2,128)(2,1)} %param.21) | copy-start | bytes 6148
  80.3 3.8 %copy-start.4 = (bf16[2,512]{1,0:T(2,128)(2,1)S(1)}, bf16[2,512]{1,0:T(2,128)(2,1)}, u32[]{:S(2)}) copy-start(bf16[2,512]{1,0:T(2,128)(2,1)} %param.22) | copy-start | bytes 6148
  80.3 4.1 %copy-start.5 = (f32[2,4]{1,0:T(2,128)S(1)}, f32[2,4]{1,0:T(2,128)}, u32[]{:S(2)}) copy-start(f32[2,4]{1,0:T(2,128)} %param.24) | copy-start | bytes 100
  80.3 28.2 %all-to-all-start = ((f32[4,2,4,128,128]{4,3,2,1,0:T(8,128)}), f32[4,2,4,128,128]{4,3,2,1,0:T(8,128)S(1)}, u32[]{:S(2)}, u32[]{:S(2)}) async-start(f32[4,2,4,128,128]{4,3,2,1,0:T(8,128)} %broadcast_in_dim.51), calls=%async_computation | async-start | bytes 4194304 | tf_op jit(solution)/shard_map/all_to_all | solution.py:151
  108.5 5.1 %copy-start.2 = (bf16[2,4,32]{2,1,0:T(4,128)(2,1)S(1)}, bf16[2,4,32]{2,1,0:T(4,128)(2,1)}, u32[]{:S(2)}) copy-start(bf16[2,4,32]{2,1,0:T(4,128)(2,1)} %param.23) | copy-start | bytes 1540
  108.5 14.1 %copy-start.6 = (f32[32]{0:T(128)S(1)}, f32[32]{0:T(128)}, u32[]{:S(2)}) copy-start(f32[32]{0:T(128)} %param.25) | copy-start | bytes 388
Sparse Core Ops, SparseCore 0:
  9.6 31.8 all-gather.1
where the time goes:
time: 130 us
  waiting for transfers between devices  65 us (50%)
  matrix products  23.3 us (18%)
  between operations  14.4 us (11%)
  blocking collectives  8.86 us (7%)
  starting transfers between devices  7.41 us (6%)
  other arithmetic  5.62 us (4%)
  local copies, waits for them, and re-layouts  5.17 us (4%)
    all_gather x1, waiting for transfers between devices, local(): incoming = lax.all_gather(tokens, 'tp', axis=2, tiled=True)  31.8 us
    all_to_all x1, waiting for transfers between devices, local(): lax.all_to_all(carry_copies, 'sp', split_axis=0, concat_axis=0, tiled=True)  24.1 us
    psum x1, blocking collectives, local(): lax.psum(jnp.sum(read_raw * read_raw, axis=-1, keepdims=True), 'sp')  8.86 us
    all_to_all x1, waiting for transfers between devices, local(): lax.all_to_all(write_parts, 'sp', split_axis=0, concat_axis=0, tiled=True)  8.45 us
    dot_general x1, matrix products, local(): jnp.dot(flat_rows, key_matrix, preferred_element_type=jnp.float32)  4.21 us
    dot_general x6, matrix products, nilpotent_inverse(): jnp.einsum('...ij,...jk->...ik', result, powered, precision=exact_mode)  3.89 us
    all_to_all x1, starting transfers between devices, local(): lax.all_to_all(carry_copies, 'sp', split_axis=0, concat_axis=0, tiled=True)  3.74 us
    dot_general x4, matrix products, fold_step(): jnp.einsum('shij,shje->shie', block_map[0], current, precision=exact_mode)  3.69 us
  transfers between devices with their start and end apart: 3, of which 3 were waited for; matrix products, arithmetic and copies ran while one was open for 2% of the time, Pallas kernels for 0%

commit v1 on v0

--- a/solution.py
+++ b/solution.py
@@ -84,7 +84,8 @@
     strength_cols = lax.dynamic_slice_in_dim(gate_matrix, all_heads + first_head, local_heads, 1)
     gate_cols = jnp.concatenate([decay_cols, strength_cols], axis=1)
     row_count = sequences * positions
-    incoming = lax.all_gather(tokens, "tp", axis=2, tiled=True)
+    parts = lax.all_gather(tokens, "tp", axis=0, tiled=False)
+    incoming = jnp.concatenate(parts, axis=2)
     span_width = incoming.shape[2]
     flat_rows = incoming.reshape(row_count, span_width)
     products = lax.optimization_barrier(

time: 130 us -> 137 us (1.054)
  local copies, waits for them, and re-layouts: 5.17 us -> 10.6 us
  other arithmetic: 5.62 us -> 9.28 us
  matrix products: 23.3 us -> 20.3 us
    add x4, other arithmetic: 0.13 us -> 3.76 us  [fold_step(): return (moved + block_map[1], None)]
    dot_general x1, matrix products: 4.21 us -> 1.24 us  [local(): jnp.dot(flat_rows, key_matrix, preferred_element_type=jnp.float32)]
    all_gather x0 -> x1, local copies, waits for them, and re-layouts: none -> 2.75 us  [local(): parts = lax.all_gather(tokens, 'tp', axis=0, tiled=False)]
    unnamed x16 -> x19, local copies, waits for them, and re-layouts: 0.5 us -> 3.18 us
where the time goes in v1:
time: 137 us; the launch traced here: 136 us
  waiting for transfers between devices  65 us (47%)
  matrix products  20.3 us (15%)
  between operations  14.4 us (11%)
  local copies, waits for them, and re-layouts  10.6 us (8%)
  other arithmetic  9.28 us (7%)
  blocking collectives  8.86 us (6%)
  starting transfers between devices  7.43 us (5%)
    all_gather x1, waiting for transfers between devices, local(): parts = lax.all_gather(tokens, 'tp', axis=0, tiled=False)  31.7 us
    all_to_all x1, waiting for transfers between devices, local(): lax.all_to_all(carry_copies, 'sp', split_axis=0, concat_axis=0, tiled=True)  24.1 us
    psum x1, blocking collectives, local(): lax.psum(jnp.sum(read_raw * read_raw, axis=-1, keepdims=True), 'sp')  8.86 us
    all_to_all x1, waiting for transfers between devices, local(): lax.all_to_all(write_parts, 'sp', split_axis=0, concat_axis=0, tiled=True)  8.44 us
    dot_general x6, matrix products, nilpotent_inverse(): jnp.einsum('...ij,...jk->...ik', result, powered, precision=exact_mode)  3.89 us
    add x4, other arithmetic, fold_step(): return (moved + block_map[1], None)  3.76 us
    all_to_all x1, starting transfers between devices, local(): lax.all_to_all(carry_copies, 'sp', split_axis=0, concat_axis=0, tiled=True)  3.75 us
    dot_general x4, matrix products, fold_step(): jnp.einsum('shij,shje->shie', block_map[0], current, precision=exact_mode)  3.69 us
  transfers between devices with their start and end apart: 3, of which 3 were waited for; matrix products, arithmetic and copies ran while one was open for 2% of the time, Pallas kernels for 0%

profile of v1, /device:TPU:0, one launch (start us, length us, event | category | flops | bytes accessed | tf_op | source)
XLA Modules:
  0.0 136.2 jit_solution(17599702234709158050)
XLA Ops:
  8.8 0.9 constant_dynamic-slice_fusion.2
  9.7 31.7 %all-gather.3.cloned.1.call-done = bf16[16,128,512]{2,1,0:T(8,128)(2,1)} async-done(((bf16[2,128,512]{2,1,0:T(8,128)(2,1)}), bf16[16,128,512]{2,1,0:T(8,128)(2,1)}) %all-gather.3.cloned.1.call-update) | async-done | bytes 2097168 | tf_op jit(solution)/shard_map/all_gather | solution.py:87
  41.5 2.8 %copy.28 = bf16[8,2,128,512]{3,0,2,1:T(8,128)(2,1)S(1)} copy(bf16[8,2,128,512]{3,2,1,0:T(8,128)(2,1)} %bitcast.104) | data formatting | bytes 4194304 | tf_op jit(solution)/shard_map/all_gather | solution.py:87
  44.2 0.9 copy.46
  45.2 1.3 copy-done.7
  46.4 1.2 fusion.52
  47.7 0.9 copy-done.8
  48.6 1.2 fusion.53
  50.7 1.1 reduce_window_sum.11
  53.5 1.0 fusion.22
  57.7 0.7 fusion.38
  63.3 4.5 %while.21 = (s32[]{:T(128)}, f32[2,4,128,256]{3,2,1,0:T(8,128)S(1)}, f32[2,2,4]{2,1,0:T(2,128)S(1)}, f32[2,2,4,64,128]{4,3,0,2,1:T(8,128)S(1)}, f32[2,2,4,64,128...) while((s32[]{:T(128)}, f32[2,4,128,256]{3,2,1,0:T(8,128)S(1)}, ...), condition=%wide.region_3.4_spmd, body=%wide.region_2.3_spmd.sunk | while | flops 403308544 | bytes 7602365 | solution.py:145
  63.5 0.7 fusion.107
  64.3 1.1 fusion.108
  65.7 0.7 fusion.107
  66.4 1.1 fusion.108
  68.2 0.8 copy.40
  69.0 3.6 %all-to-all-start.1 = ((f32[4,2,4,128,32]{3,4,2,1,0:T(8,128)}), f32[4,2,4,128,32]{3,4,2,1,0:T(8,128)S(1)}, u32[]{:S(2)}, u32[]{:S(2)}) async-start(f32[4,2,4,128,32]{3,4,2,1,0:T(8,128)} %copy.40), calls=%async_computation.1 | async-start | bytes 1048576 | tf_op jit(solution)/shard_map/all_to_all | solution.py:153
  72.7 8.4 %all-to-all-done.1 = f32[4,2,4,128,32]{3,4,2,1,0:T(8,128)S(1)} async-done(((f32[4,2,4,128,32]{3,4,2,1,0:T(8,128)}), f32[4,2,4,128,32]{3,4,2,1,0:T(8,128)S(1)}, u32[]{:S(2)}, u32[]{:S(2)}) %all-to-all-start.1) | async-done | bytes 524320 | tf_op jit(solution)/shard_map/all_to_all | solution.py:153
  81.2 1.6 %broadcast_in_dim.51 = f32[4,2,4,128,128]{4,3,2,1,0:T(8,128)} broadcast(f32[2,4,128,128]{3,2,1,0:T(8,128)S(1)} %slice.18), dimensions={1,2,3,4} | broadcast | bytes 2621440 | tf_op jit(solution)/shard_map/broadcast_in_dim | solution.py:148
  82.8 3.8 %all-to-all-start = ((f32[4,2,4,128,128]{4,3,2,1,0:T(8,128)}), f32[4,2,4,128,128]{4,3,2,1,0:T(8,128)S(1)}, u32[]{:S(2)}, u32[]{:S(2)}) async-start(f32[4,2,4,128,128]{4,3,2,1,0:T(8,128)} %broadcast_in_dim.51), calls=%async_computation | async-start | bytes 4194304 | tf_op jit(solution)/shard_map/all_to_all | solution.py:152
  86.9 24.1 %all-to-all-done = f32[4,2,4,128,128]{4,3,2,1,0:T(8,128)S(1)} async-done(((f32[4,2,4,128,128]{4,3,2,1,0:T(8,128)}), f32[4,2,4,128,128]{4,3,2,1,0:T(8,128)S(1)}, u32[]{:S(2)}, u32[]{:S(2)}) %all-to-all-start) | async-done | bytes 2097184 | tf_op jit(solution)/shard_map/all_to_all | solution.py:152
  111.0 7.5 %while.22 = (s32[]{:T(128)}, f32[2,4,128,32]{2,3,1,0:T(8,128)S(1)}, f32[4,2,4,128,128]{4,3,2,1,0:T(8,128)S(1)}, f32[4,2,4,128,32]{3,4,2,1,0:T(8,128)}, s32[]{:T(128)}, /*index=5*/s32[]{:T(128)}) while((s32[]{:T(128)}, f32[2,4,128,32]{2,3,1,0:T(8,128)S(1)}, f32[4,2,4,128,128]{4,3,2,1,0:T(8,128)S(1)}, ...), condition=%wide.region_5.6_spmd.clone, body=%wide.region_4.5_spmd.clone.sunk | while | flops 50397184 | bytes 1179735 | solution.py:162
  111.0 0.9 fusion.112
  111.9 0.9 bitcast_add_fusion.2
  112.8 0.9 fusion.112
  113.8 0.9 bitcast_add_fusion.2
  114.7 0.9 fusion.112
  115.6 0.9 bitcast_add_fusion.2
  116.6 0.9 fusion.112
  117.5 0.9 bitcast_add_fusion.2
  119.8 8.9 %psum.7 = f32[2,4,1]{1,0,2:T(2,128)S(1)} all-reduce(f32[2,4,1]{1,0,2:T(2,128)S(1)} %bitcast.117), channel_id=1, replica_groups=mesh['sp'=4,'tp'=8] {'sp'}, use_global_device_ids=true, to_apply=%region_9.10 | all-reduce | flops 8 | bytes 64 | tf_op jit(solution)/shard_map/psum | solution.py:174
  (79 shorter events, 15.5 us)
Async XLA Ops:
  7.2 34.3 %all-gather.3.cloned.1.call-start = ((), (), s32[]{:S(2)}) async-start(), calls=%async_computation.2 | async-start | bytes 2359296 | tf_op jit(solution)/shard_map/all_gather | solution.py:87
  44.2 2.2 %copy-start.7 = (bf16[4096,512]{1,0:T(8,128)(2,1)S(1)}, bf16[4096,512]{1,0:T(8,128)(2,1)}, u32[]{:S(2)}) copy-start(bf16[4096,512]{1,0:T(8,128)(2,1)} %param.16) | copy-start | bytes 12582916
  46.4 2.2 %copy-start.8 = (bf16[4096,512]{1,0:T(8,128)(2,1)S(1)}, bf16[4096,512]{1,0:T(8,128)(2,1)}, u32[]{:S(2)}) copy-start(bf16[4096,512]{1,0:T(8,128)(2,1)} %param.17) | copy-start | bytes 12582916
  49.9 0.7 copy-start.3
  69.0 12.1 %all-to-all-start.1 = ((f32[4,2,4,128,32]{3,4,2,1,0:T(8,128)}), f32[4,2,4,128,32]{3,4,2,1,0:T(8,128)S(1)}, u32[]{:S(2)}, u32[]{:S(2)}) async-start(f32[4,2,4,128,32]{3,4,2,1,0:T(8,128)} %copy.40), calls=%async_computation.1 | async-start | bytes 1048576 | tf_op jit(solution)/shard_map/all_to_all | solution.py:153
  81.2 1.6 %copy-start = (f32[4,2,4,128,32]{3,4,2,1,0:T(8,128)}, f32[4,2,4,128,32]{3,4,2,1,0:T(8,128)S(1)}, u32[]{:S(2)}) copy-start(f32[4,2,4,128,32]{3,4,2,1,0:T(8,128)S(1)} %all-to-all-done.1) | copy-start | bytes 1572868
  82.8 3.8 %copy-start.1 = (bf16[2,512]{1,0:T(2,128)(2,1)S(1)}, bf16[2,512]{1,0:T(2,128)(2,1)}, u32[]{:S(2)}) copy-start(bf16[2,512]{1,0:T(2,128)(2,1)} %param.21) | copy-start | bytes 6148
  82.8 3.8 %copy-start.4 = (bf16[2,512]{1,0:T(2,128)(2,1)S(1)}, bf16[2,512]{1,0:T(2,128)(2,1)}, u32[]{:S(2)}) copy-start(bf16[2,512]{1,0:T(2,128)(2,1)} %param.22) | copy-start | bytes 6148
  82.8 4.1 %copy-start.5 = (f32[2,4]{1,0:T(2,128)S(1)}, f32[2,4]{1,0:T(2,128)}, u32[]{:S(2)}) copy-start(f32[2,4]{1,0:T(2,128)} %param.24) | copy-start | bytes 100
  82.8 28.2 %all-to-all-start = ((f32[4,2,4,128,128]{4,3,2,1,0:T(8,128)}), f32[4,2,4,128,128]{4,3,2,1,0:T(8,128)S(1)}, u32[]{:S(2)}, u32[]{:S(2)}) async-start(f32[4,2,4,128,128]{4,3,2,1,0:T(8,128)} %broadcast_in_dim.51), calls=%async_computation | async-start | bytes 4194304 | tf_op jit(solution)/shard_map/all_to_all | solution.py:152
  111.0 8.7 %copy-start.2 = (bf16[2,4,32]{2,1,0:T(4,128)(2,1)S(1)}, bf16[2,4,32]{2,1,0:T(4,128)(2,1)}, u32[]{:S(2)}) copy-start(bf16[2,4,32]{2,1,0:T(4,128)(2,1)} %param.23) | copy-start | bytes 1540
  111.0 17.7 %copy-start.6 = (f32[32]{0:T(128)S(1)}, f32[32]{0:T(128)}, u32[]{:S(2)}) copy-start(f32[32]{0:T(128)} %param.25) | copy-start | bytes 388
Sparse Core Ops, SparseCore 0:
  9.6 31.8 all-gather.2
